TPU v7x, 512 devices: a whole 4x8x8 slice. The times are simulated.
512 devices in a mesh: sp: 64 (over z, y), tp: 8 (over x, core).
Axes of the slice: x: 4, y: 8, z: 8, core: 2. Of those that a mesh axis runs over, the one named last changes fastest.
Arguments:
- queries: bfloat16 [16384, 512], P('sp', 'tp'), may hold values from -8 to 8
- keys: bfloat16 [16384, 512], P('sp', 'tp'), may hold values from -8 to 8
- values: bfloat16 [16384, 512], P('sp', 'tp'), may hold values from -6 to 6
- score_shift: float32 [8], P('tp'), may hold values from 3 to 20
- resid: bfloat16 [16384, 2048], P(('sp', 'tp')), may hold values from -6 to 6
- w_out: bfloat16 [512, 2048], replicated, may hold values from -0.25 to 0.25
- gain_mix: float32 [2048], replicated, may hold values from 0.1 to 1.9
- gain_pre: float32 [2048], replicated, may hold values from 0.1 to 1.9
- w_gate: bfloat16 [2048, 5632], P('sp', 'tp'), may hold values from -0.125 to 0.125
- w_up: bfloat16 [2048, 5632], P('sp', 'tp'), may hold values from -0.125 to 0.125
- conv_gate: float32 [3, 5632], P(None, 'tp'), may hold values from -3 to 3
- conv_up: float32 [3, 5632], P(None, 'tp'), may hold values from -3 to 3
- w_down: bfloat16 [5632, 2048], P('tp', 'sp'), may hold values from -0.078125 to 0.078125
- gain_post: float32 [2048], replicated, may hold values from 0.1 to 1.9
Outputs:
- result: bfloat16 [16384, 2048], P(('sp', 'tp'))
All inputs are finite; a program needn't handle non-finite values.
Results may differ from a plain program's by a relative error of at most 0.017.
Values may be sent and summed in bfloat16 or wider, within the bound.
A program may use at most 64 MiB of HBM per device.

v0:
```python
import jax
import jax.numpy as jnp
from jax import lax
from jax.sharding import PartitionSpec as P

HEAD_DIM = 64
KERNEL = 3


def side_by_side(arrays, axis, dim, along):
    widths = [a.shape[along] for a in arrays]
    both = jnp.concatenate(arrays, axis=along)
    out = lax.all_gather(both, axis, axis=dim, tiled=True)
    return tuple(jnp.split(out, [sum(widths[:k]) for k in range(1, len(widths))], axis=along))


def laid_out(parts, dim):
    parts = jnp.moveaxis(parts, 0, dim)
    lengths = parts.shape
    return parts.reshape(*lengths[:dim], lengths[dim] * lengths[dim + 1], *lengths[dim + 2 :])


def from_everyone(x, axis):
    length = lax.axis_size(axis)
    return lax.all_to_all(jnp.broadcast_to(x[None], (length, *x.shape)), axis, 0, 0, tiled=True)


def gathered_copies(x, axis, dim):
    return laid_out(from_everyone(x, axis), dim)


def from_behind(x, axis, by):
    length = lax.axis_size(axis)
    pairs = [(i, i + by) for i in range(length) if 0 <= i + by < length]
    return lax.ppermute(x, axis, pairs)


def split_up(x, dim, length):
    before, after = (x.shape[:dim], x.shape[dim + 1 :])
    return jnp.moveaxis(x.reshape(*before, length, -1, *after), dim, 0)


def sum_at_owner(x, axis, dim):
    parts = split_up(x, dim, lax.axis_size(axis))
    arrived = lax.all_to_all(parts, axis, split_axis=0, concat_axis=0, tiled=True)
    return arrived.astype(jnp.float32).sum(axis=0)


def rms_scale(values_in):
    return values_in * lax.rsqrt(jnp.mean(values_in * values_in, axis=-1, keepdims=True) + 1e-06)


def collect_weights(w_gate, w_up, w_down):
    gate_whole, up_whole = side_by_side((w_gate, w_up), "sp", 0, 1)
    down_whole = lax.all_gather(w_down, "sp", axis=1, tiled=True)
    return (gate_whole, up_whole, down_whole)


def stick_attention(queries, key_whole, value_whole, score_shift):
    tok_rows = queries.shape[0]
    local_heads = queries.shape[1] // HEAD_DIM
    total = key_whole.shape[0]
    shards = total // tok_rows
    group = max(
        (
            factor
            for factor in range(1, shards + 1)
            if shards % factor == 0 and factor * tok_rows <= max(2048, tok_rows)
        )
    )
    span = group * tok_rows
    offset = lax.axis_index("sp") * tok_rows
    query_heads = queries.reshape(tok_rows, local_heads, HEAD_DIM)
    key_heads = key_whole.reshape(total, local_heads, HEAD_DIM)
    value_heads = value_whole.reshape(total, local_heads, HEAD_DIM)
    query_pos = offset + jnp.arange(tok_rows, dtype=jnp.int32)
    last_block = (offset + tok_rows - 1) // span

    def visit(turn, carry):
        accum, tail = carry
        block_start = (last_block - turn) * span
        key_block = lax.dynamic_slice_in_dim(key_heads, block_start, span, 0)
        value_block = lax.dynamic_slice_in_dim(value_heads, block_start, span, 0)
        scores = jnp.einsum(
            "qhd,khd->hqk", query_heads, key_block, preferred_element_type=jnp.float32
        )
        scores = scores * HEAD_DIM ** (-0.5) - score_shift[:, None, None]
        key_pos = block_start + jnp.arange(span, dtype=jnp.int32)
        causal = (key_pos[None, :] < query_pos[:, None])[None, :, :]
        log_keep = jnp.where(causal, -jax.nn.softplus(scores), 0.0)
        later = lax.cumsum(log_keep, axis=2, reverse=True) - log_keep
        weights = jnp.where(
            causal, jnp.exp(jax.nn.log_sigmoid(scores) + later + tail[:, :, None]), 0.0
        ).astype(jnp.bfloat16)
        accum = accum + jnp.einsum(
            "hqk,khd->hqd", weights, value_block, preferred_element_type=jnp.float32
        )
        return (accum, tail + jnp.sum(log_keep, axis=2))

    start_carry = (
        jnp.zeros((local_heads, tok_rows, HEAD_DIM), jnp.float32),
        jnp.zeros((local_heads, tok_rows), jnp.float32),
    )
    accum, _ = lax.fori_loop(0, last_block + 1, visit, start_carry)
    return accum.transpose(1, 0, 2).reshape(tok_rows, local_heads * HEAD_DIM).astype(jnp.bfloat16)


def local(
    queries,
    keys,
    values,
    score_shift,
    resid,
    w_out,
    gain_mix,
    gain_pre,
    w_gate,
    w_up,
    conv_gate,
    conv_up,
    w_down,
    gain_post,
):
    gate_whole, up_whole, down_whole = collect_weights(w_gate, w_up, w_down)
    key_whole, value_whole = side_by_side((keys, values), "sp", 0, 1)
    attended = stick_attention(queries, key_whole, value_whole, score_shift)
    head_rows = lax.all_to_all(attended, "tp", split_axis=0, concat_axis=1, tiled=True)
    mixed = jnp.dot(head_rows, w_out, preferred_element_type=jnp.float32).astype(jnp.bfloat16)
    middle = (resid.astype(jnp.float32) + gain_mix * rms_scale(mixed.astype(jnp.float32))).astype(
        jnp.bfloat16
    )
    normed = (gain_pre * rms_scale(middle.astype(jnp.float32))).astype(jnp.bfloat16)
    piece = gathered_copies(normed, "tp", 0)
    gate_part = jnp.dot(piece, gate_whole, preferred_element_type=jnp.float32).astype(jnp.bfloat16)
    up_part = jnp.dot(piece, up_whole, preferred_element_type=jnp.float32).astype(jnp.bfloat16)
    projected = jnp.concatenate([gate_part, up_part], axis=1)
    tok_rows = projected.shape[0]
    local_units = projected.shape[1] // 2
    edge = from_behind(projected[tok_rows - (KERNEL - 1) :], "sp", 1)
    extended = jnp.concatenate([edge, projected], axis=0).astype(jnp.float32)
    taps = jnp.concatenate([conv_gate, conv_up], axis=1)
    convolved = taps[0] * extended[0:tok_rows]
    for tap in range(1, KERNEL):
        convolved = convolved + taps[tap] * extended[tap : tap + tok_rows]
    hidden = (jax.nn.silu(convolved[:, :local_units]) * convolved[:, local_units:]).astype(
        jnp.bfloat16
    )
    summed = sum_at_owner(
        jnp.dot(hidden, down_whole, preferred_element_type=jnp.float32).astype(jnp.bfloat16),
        "tp",
        0,
    )
    ffn_out = summed.astype(jnp.bfloat16)
    return (middle.astype(jnp.float32) + gain_post * rms_scale(ffn_out.astype(jnp.float32))).astype(
        jnp.bfloat16
    )


def solution(mesh):
    in_specs = (
        P("sp", "tp"),
        P("sp", "tp"),
        P("sp", "tp"),
        P("tp"),
        P(("sp", "tp"), None),
        P(),
        P(),
        P(),
        P("sp", "tp"),
        P("sp", "tp"),
        P(None, "tp"),
        P(None, "tp"),
        P("tp", "sp"),
        P(),
    )
    out_specs = P(("sp", "tp"), None)
    return jax.shard_map(local, mesh=mesh, in_specs=in_specs, out_specs=out_specs, check_vma=False)
```

profile of v0, /device:TPU:448, one launch (start us, length us, event | category | flops | bytes accessed | tf_op | source)
XLA Modules:
  0.0 331.4 jit_solution(313989612567962187)
XLA Ops:
  10.5 88.7 %all-gather.4.cloned.1.call-done = bf16[16384,128]{0,1:T(8,128)(2,1)} async-done(((bf16[256,128]{0,1:T(8,128)(2,1)}), bf16[16384,128]{0,1:T(8,128)(2,1)}) %all-gather.4.cloned.1.call-update) | async-done | bytes 4194320 | tf_op jit(solution)/shard_map/all_gather | solution.py:13
  103.8 146.1 %while.13 = (s32[]{:T(128)}, f32[1,256,64]{1,2,0:T(8,128)S(1)}, f32[1,256]{1,0:T(1,128)S(1)}, s32[]{:T(128)}, s32[]{:T(128)}, /*index=5*/bf16[16384,1,64]{0,2,1:...) while((s32[]{:T(128)}, f32[1,256,64]{1,2,0:T(8,128)S(1)}, ...), condition=%wide.region_4.5_spmd.clone, body=%wide.region_0.4_spmd.clone.sunk | while | flops 219236352 | bytes 19711708 | solution.py:104
  103.8 4.6 %fusion.62 = (f32[256]{0:T(256)S(1)}, f32[256,2048]{0,1:T(8,128)S(1)}, f32[256,2048]{0,1:T(8,128)}) fusion(s32[256]{0:T(256)S(1)} %iota_add_fusion.4, s32[2048]{0:T(1024)S(1)} %iota_add_fusion.5, f32[]{:T(128)} %bitcast.72, bf16[256,1,64]{0,2,1:T(8,128)(2,1)S(1)} %get-tuple-element.219, bf16[16384,1,64]{0,2,1:T(8,128)(2,1)} %get-tuple-element.218, ...), kind=kOutput, calls=%fused_computation.31.clone.1 | convolution fusion | flops 73400064 | bytes 4499972 | tf_op jit(solution)/shard_map/while/body/qhd,khd->hqk/dot_general | solution.py:84
  108.4 5.0 %fusion.63 = f32[1,256,16,128]{1,2,3,0:T(8,128)S(1)} fusion(f32[1,256,16,128]{1,3,2,0:T(8,128)S(1)} %bitcast.76), kind=kOutput, calls=%fused_computation.16.clone.1 | output fusion | flops 66584576 | bytes 4194304 | tf_op jit(solution)/shard_map/reduce-window
  116.1 4.6 %fusion.64 = bf16[256,2048]{0,1:T(8,128)(2,1)S(1)} fusion(f32[1,256,16,128]{1,3,2,0:T(8,128)} %copy.29, f32[256,2048]{0,1:T(8,128)} %get-tuple-element.181, f32[256]{0:T(256)S(1)} %bitcast.82, f32[256,16]{0,1:T(8,128)S(1)} %slice_bitcast_fusion.7, s32[256]{0:T(256)S(1)} %iota_add_fusion.4, s32[2048]{0:T(1024)S(1)} %iota_add_fusion.5), kind=kLoop, calls=%fused_computation.8.clone.1 | loop fusion | flops 12058624 | bytes 5269504 | tf_op jit(solution)/shard_map/while/body/convert_element_type | solution.py:94
  126.6 5.0 %fusion.63 = f32[1,256,16,128]{1,2,3,0:T(8,128)S(1)} fusion(f32[1,256,16,128]{1,3,2,0:T(8,128)S(1)} %bitcast.76), kind=kOutput, calls=%fused_computation.16.clone.1 | output fusion | flops 66584576 | bytes 4194304 | tf_op jit(solution)/shard_map/reduce-window
  134.4 4.6 %fusion.64 = bf16[256,2048]{0,1:T(8,128)(2,1)S(1)} fusion(f32[1,256,16,128]{1,3,2,0:T(8,128)} %copy.29, f32[256,2048]{0,1:T(8,128)} %get-tuple-element.181, f32[256]{0:T(256)S(1)} %bitcast.82, f32[256,16]{0,1:T(8,128)S(1)} %slice_bitcast_fusion.7, s32[256]{0:T(256)S(1)} %iota_add_fusion.4, s32[2048]{0:T(1024)S(1)} %iota_add_fusion.5), kind=kLoop, calls=%fused_computation.8.clone.1 | loop fusion | flops 12058624 | bytes 5269504 | tf_op jit(solution)/shard_map/while/body/convert_element_type | solution.py:94
  144.9 5.0 %fusion.63 = f32[1,256,16,128]{1,2,3,0:T(8,128)S(1)} fusion(f32[1,256,16,128]{1,3,2,0:T(8,128)S(1)} %bitcast.76), kind=kOutput, calls=%fused_computation.16.clone.1 | output fusion | flops 66584576 | bytes 4194304 | tf_op jit(solution)/shard_map/reduce-window
  152.6 4.6 %fusion.64 = bf16[256,2048]{0,1:T(8,128)(2,1)S(1)} fusion(f32[1,256,16,128]{1,3,2,0:T(8,128)} %copy.29, f32[256,2048]{0,1:T(8,128)} %get-tuple-element.181, f32[256]{0:T(256)S(1)} %bitcast.82, f32[256,16]{0,1:T(8,128)S(1)} %slice_bitcast_fusion.7, s32[256]{0:T(256)S(1)} %iota_add_fusion.4, s32[2048]{0:T(1024)S(1)} %iota_add_fusion.5), kind=kLoop, calls=%fused_computation.8.clone.1 | loop fusion | flops 12058624 | bytes 5269504 | tf_op jit(solution)/shard_map/while/body/convert_element_type | solution.py:94
  163.1 5.0 %fusion.63 = f32[1,256,16,128]{1,2,3,0:T(8,128)S(1)} fusion(f32[1,256,16,128]{1,3,2,0:T(8,128)S(1)} %bitcast.76), kind=kOutput, calls=%fused_computation.16.clone.1 | output fusion | flops 66584576 | bytes 4194304 | tf_op jit(solution)/shard_map/reduce-window
  170.9 4.7 %fusion.64 = bf16[256,2048]{0,1:T(8,128)(2,1)S(1)} fusion(f32[1,256,16,128]{1,3,2,0:T(8,128)} %copy.29, f32[256,2048]{0,1:T(8,128)} %get-tuple-element.181, f32[256]{0:T(256)S(1)} %bitcast.82, f32[256,16]{0,1:T(8,128)S(1)} %slice_bitcast_fusion.7, s32[256]{0:T(256)S(1)} %iota_add_fusion.4, s32[2048]{0:T(1024)S(1)} %iota_add_fusion.5), kind=kLoop, calls=%fused_computation.8.clone.1 | loop fusion | flops 12058624 | bytes 5269504 | tf_op jit(solution)/shard_map/while/body/convert_element_type | solution.py:94
  176.9 4.6 %fusion.62 = (f32[256]{0:T(256)S(1)}, f32[256,2048]{0,1:T(8,128)S(1)}, f32[256,2048]{0,1:T(8,128)}) fusion(s32[256]{0:T(256)S(1)} %iota_add_fusion.4, s32[2048]{0:T(1024)S(1)} %iota_add_fusion.5, f32[]{:T(128)} %bitcast.72, bf16[256,1,64]{0,2,1:T(8,128)(2,1)S(1)} %get-tuple-element.219, bf16[16384,1,64]{0,2,1:T(8,128)(2,1)} %get-tuple-element.218, ...), kind=kOutput, calls=%fused_computation.31.clone.1 | convolution fusion | flops 73400064 | bytes 4499972 | tf_op jit(solution)/shard_map/while/body/qhd,khd->hqk/dot_general | solution.py:84
  181.5 5.0 %fusion.63 = f32[1,256,16,128]{1,2,3,0:T(8,128)S(1)} fusion(f32[1,256,16,128]{1,3,2,0:T(8,128)S(1)} %bitcast.76), kind=kOutput, calls=%fused_computation.16.clone.1 | output fusion | flops 66584576 | bytes 4194304 | tf_op jit(solution)/shard_map/reduce-window
  189.2 4.6 %fusion.64 = bf16[256,2048]{0,1:T(8,128)(2,1)S(1)} fusion(f32[1,256,16,128]{1,3,2,0:T(8,128)} %copy.29, f32[256,2048]{0,1:T(8,128)} %get-tuple-element.181, f32[256]{0:T(256)S(1)} %bitcast.82, f32[256,16]{0,1:T(8,128)S(1)} %slice_bitcast_fusion.7, s32[256]{0:T(256)S(1)} %iota_add_fusion.4, s32[2048]{0:T(1024)S(1)} %iota_add_fusion.5), kind=kLoop, calls=%fused_computation.8.clone.1 | loop fusion | flops 12058624 | bytes 5269504 | tf_op jit(solution)/shard_map/while/body/convert_element_type | solution.py:94
  199.7 5.0 %fusion.63 = f32[1,256,16,128]{1,2,3,0:T(8,128)S(1)} fusion(f32[1,256,16,128]{1,3,2,0:T(8,128)S(1)} %bitcast.76), kind=kOutput, calls=%fused_computation.16.clone.1 | output fusion | flops 66584576 | bytes 4194304 | tf_op jit(solution)/shard_map/reduce-window
  207.4 4.6 %fusion.64 = bf16[256,2048]{0,1:T(8,128)(2,1)S(1)} fusion(f32[1,256,16,128]{1,3,2,0:T(8,128)} %copy.29, f32[256,2048]{0,1:T(8,128)} %get-tuple-element.181, f32[256]{0:T(256)S(1)} %bitcast.82, f32[256,16]{0,1:T(8,128)S(1)} %slice_bitcast_fusion.7, s32[256]{0:T(256)S(1)} %iota_add_fusion.4, s32[2048]{0:T(1024)S(1)} %iota_add_fusion.5), kind=kLoop, calls=%fused_computation.8.clone.1 | loop fusion | flops 12058624 | bytes 5269504 | tf_op jit(solution)/shard_map/while/body/convert_element_type | solution.py:94
  217.9 5.0 %fusion.63 = f32[1,256,16,128]{1,2,3,0:T(8,128)S(1)} fusion(f32[1,256,16,128]{1,3,2,0:T(8,128)S(1)} %bitcast.76), kind=kOutput, calls=%fused_computation.16.clone.1 | output fusion | flops 66584576 | bytes 4194304 | tf_op jit(solution)/shard_map/reduce-window
  225.7 4.6 %fusion.64 = bf16[256,2048]{0,1:T(8,128)(2,1)S(1)} fusion(f32[1,256,16,128]{1,3,2,0:T(8,128)} %copy.29, f32[256,2048]{0,1:T(8,128)} %get-tuple-element.181, f32[256]{0:T(256)S(1)} %bitcast.82, f32[256,16]{0,1:T(8,128)S(1)} %slice_bitcast_fusion.7, s32[256]{0:T(256)S(1)} %iota_add_fusion.4, s32[2048]{0:T(1024)S(1)} %iota_add_fusion.5), kind=kLoop, calls=%fused_computation.8.clone.1 | loop fusion | flops 12058624 | bytes 5269504 | tf_op jit(solution)/shard_map/while/body/convert_element_type | solution.py:94
  236.2 5.0 %fusion.63 = f32[1,256,16,128]{1,2,3,0:T(8,128)S(1)} fusion(f32[1,256,16,128]{1,3,2,0:T(8,128)S(1)} %bitcast.76), kind=kOutput, calls=%fused_computation.16.clone.1 | output fusion | flops 66584576 | bytes 4194304 | tf_op jit(solution)/shard_map/reduce-window
  243.9 4.6 %fusion.64 = bf16[256,2048]{0,1:T(8,128)(2,1)S(1)} fusion(f32[1,256,16,128]{1,3,2,0:T(8,128)} %copy.29, f32[256,2048]{0,1:T(8,128)} %get-tuple-element.181, f32[256]{0:T(256)S(1)} %bitcast.82, f32[256,16]{0,1:T(8,128)S(1)} %slice_bitcast_fusion.7, s32[256]{0:T(256)S(1)} %iota_add_fusion.4, s32[2048]{0:T(1024)S(1)} %iota_add_fusion.5), kind=kLoop, calls=%fused_computation.8.clone.1 | loop fusion | flops 12058624 | bytes 5269504 | tf_op jit(solution)/shard_map/while/body/convert_element_type | solution.py:94
  250.1 9.5 %all_to_all.26 = bf16[8,2,1024]{2,1,0:T(2,128)(2,1)S(1)} all-to-all(bf16[8,2,1024]{2,1,0:T(2,128)(2,1)S(1)} %reshape.137), channel_id=1, replica_groups=mesh['sp'=64,'tp'=8] {'tp'}, dimensions={0} | all-to-all | bytes 65536 | tf_op jit(solution)/shard_map/all_to_all | solution.py:127
  261.6 18.4 %all_to_all.27 = bf16[8,32,2048]{2,1,0:T(8,128)(2,1)S(1)} all-to-all(bf16[8,32,2048]{2,1,0:T(8,128)(2,1)S(1)} %broadcast_in_dim.16), channel_id=1, replica_groups=mesh['sp'=64,'tp'=8] {'tp'}, dimensions={0} | all-to-all | bytes 2097152 | tf_op jit(solution)/shard_map/all_to_all | solution.py:25
  289.5 10.7 %collective-permute-done = bf16[2,1408]{0,1:T(8,128)(2,1)S(1)} collective-permute-done((bf16[2,1408]{0,1:T(8,128)(2,1)S(1)}, bf16[2,1408]{0,1:T(8,128)(2,1)S(1)}, u32[]{:S(2)}, u32[]{:S(2)}) %collective-permute-start) | collective-permute-done | bytes 5664 | tf_op jit(solution)/shard_map/ppermute | solution.py:35
  305.3 18.5 %all_to_all.28 = bf16[8,32,2048]{2,1,0:T(8,128)(2,1)S(1)} all-to-all(bf16[8,32,2048]{2,1,0:T(8,128)(2,1)S(1)} %bitcast.79), channel_id=1, replica_groups=mesh['sp'=64,'tp'=8] {'tp'}, dimensions={0} | all-to-all | bytes 2097152 | tf_op jit(solution)/shard_map/all_to_all | solution.py:45
  (128 shorter events, 85.1 us)
Async XLA Ops:
  6.5 253.4 %copy-start = (bf16[512,2048]{1,0:T(8,128)(2,1)S(1)}, bf16[512,2048]{1,0:T(8,128)(2,1)}, u32[]{:S(2)}) copy-start(bf16[512,2048]{1,0:T(8,128)(2,1)} %param.21) | copy-start | bytes 6291460
  6.5 92.7 %all-gather.4.cloned.1.call-start = ((), (), s32[]{:S(2)}) async-start(), calls=%async_computation.3 | async-start | bytes 4259840 | tf_op jit(solution)/shard_map/all_gather | solution.py:13
  8.1 271.9 %all-gather.6.cloned.1.call-start = ((), (), s32[]{:S(2)}) async-start(), calls=%async_computation.4 | async-start | bytes 5857280 | tf_op jit(solution)/shard_map/all_gather | solution.py:13
  9.7 292.6 %all-gather.8.cloned.1.call-start = ((), (), s32[]{:S(2)}) async-start(), calls=%async_computation.5 | async-start | bytes 3194880 | tf_op jit(solution)/shard_map/all_gather | solution.py:55
  10.5 93.3 %copy-start.10 = (bf16[256,64]{0,1:T(8,128)(2,1)S(1)}, bf16[256,64]{0,1:T(8,128)(2,1)}, u32[]{:S(2)}) copy-start(bf16[256,64]{0,1:T(8,128)(2,1)} %param.16) | copy-start | bytes 98308
  249.9 10.6 %copy-start.3 = (bf16[32,2048]{1,0:T(8,128)(2,1)S(1)}, bf16[32,2048]{1,0:T(8,128)(2,1)}, u32[]{:S(2)}) copy-start(bf16[32,2048]{1,0:T(8,128)(2,1)} %param.20) | copy-start | bytes 393220
  249.9 10.6 %copy-start.6 = (f32[2048]{0:T(1024)S(1)}, f32[2048]{0:T(1024)}, u32[]{:S(2)}) copy-start(f32[2048]{0:T(1024)} %param.22) | copy-start | bytes 24580
  249.9 11.5 %copy-start.7 = (f32[2048]{0:T(1024)S(1)}, f32[2048]{0:T(1024)}, u32[]{:S(2)}) copy-start(f32[2048]{0:T(1024)} %param.23) | copy-start | bytes 24580
  260.7 0.7 copy-start.1
  280.0 3.6 %copy-start.9 = (bf16[2048,1408]{1,0:T(8,128)(2,1)S(1)}, bf16[2048,1408]{1,0:T(8,128)(2,1)}, u32[]{:S(2)}) copy-start(bf16[2048,1408]{1,0:T(8,128)(2,1)} %all-gather.6.cloned.1.call-done) | copy-start | bytes 17301508
  283.6 5.8 %copy-start.4 = (f32[3,704]{1,0:T(4,128)S(1)}, f32[3,704]{1,0:T(4,128)}, u32[]{:S(2)}) copy-start(f32[3,704]{1,0:T(4,128)} %param.27) | copy-start | bytes 25348
  283.6 5.8 %copy-start.5 = (f32[3,704]{1,0:T(4,128)S(1)}, f32[3,704]{1,0:T(4,128)}, u32[]{:S(2)}) copy-start(f32[3,704]{1,0:T(4,128)} %param.26) | copy-start | bytes 25348
  286.5 13.8 %collective-permute-start = (bf16[2,1408]{0,1:T(8,128)(2,1)S(1)}, bf16[2,1408]{0,1:T(8,128)(2,1)S(1)}, u32[]{:S(2)}, u32[]{:S(2)}) collective-permute-start(bf16[2,1408]{0,1:T(8,128)(2,1)S(1)} %pad_maximum_fusion), channel_id=1, source_target_pairs={{0,8},{8,16},{16,24},{24,32},{32,40},{40,48},{48,56},{56,64},{64,7... | collective-permute-start | bytes 16904 | tf_op jit(solution)/shard_map/ppermute | solution.py:35
  305.3 18.9 %copy-start.2 = (bf16[32,2048]{1,0:T(8,128)(2,1)S(1)}, bf16[32,2048]{1,0:T(8,128)(2,1)}, u32[]{:S(2)}) copy-start(bf16[32,2048]{1,0:T(8,128)(2,1)} %copy-done.1) | copy-start | bytes 393220
  305.3 18.8 %copy-start.8 = (f32[2048]{0:T(1024)S(1)}, f32[2048]{0:T(1024)}, u32[]{:S(2)}) copy-start(f32[2048]{0:T(1024)} %param.29) | copy-start | bytes 24580
Sparse Core Ops, SparseCore 0:
  10.3 88.8 all-gather.3
  102.2 85.3 all-gather.5
  190.6 82.1 all-gather.7
where the time goes:
time: 332 us; the launch traced here: 331 us
  waiting for transfers between devices  100 us (30%)
  other arithmetic  84.9 us (26%)
  matrix products  56 us (17%)
  blocking collectives  46.4 us (14%)
  local copies, waits for them, and re-layouts  27 us (8%)
  between operations  13.3 us (4%)
    all_gather x2, waiting for transfers between devices, side_by_side(): out = lax.all_gather(both, axis, axis=dim, tiled=True)  88.7 us
    another operation x16, other arithmetic  40.8 us
    convert_element_type x8, other arithmetic, visit(): weights = jnp.where(causal, jnp.exp(jax.nn.log_sigmoid(scores) + later +...  37.1 us
    dot_general x8, matrix products, visit(): jnp.einsum('qhd,khd->hqk', query_heads, key_block, preferred_element_type...  36.4 us
    another operation x24, local copies, waits for them, and re-layouts  21 us
    all_to_all x1, blocking collectives, sum_at_owner(): lax.all_to_all(parts, axis, split_axis=0, concat_axis=0, tiled=True)  18.5 us
    all_to_all x1, blocking collectives, from_everyone(): lax.all_to_all(jnp.broadcast_to(x[None], (length, *x.shape)), axis, 0, 0,...  18.4 us
    ppermute x1, waiting for transfers between devices, from_behind(): return lax.ppermute(x, axis, pairs)  10.7 us
  transfers between devices with their start and end apart: 4, of which 2 were waited for; matrix products, arithmetic and copies ran while one was open for 49% of the time, Pallas kernels for 0%

commit v1 on v0

--- a/solution.py
+++ b/solution.py
@@ -124,7 +124,10 @@
     gate_whole, up_whole, down_whole = collect_weights(w_gate, w_up, w_down)
     key_whole, value_whole = side_by_side((keys, values), "sp", 0, 1)
     attended = stick_attention(queries, key_whole, value_whole, score_shift)
-    head_rows = lax.all_to_all(attended, "tp", split_axis=0, concat_axis=1, tiled=True)
+    head_rows = jnp.concatenate(
+        lax.all_to_all(jnp.stack(jnp.split(attended, lax.axis_size("tp"), axis=0)), "tp", 0, 0),
+        axis=1,
+    )
     mixed = jnp.dot(head_rows, w_out, preferred_element_type=jnp.float32).astype(jnp.bfloat16)
     middle = (resid.astype(jnp.float32) + gain_mix * rms_scale(mixed.astype(jnp.float32))).astype(
         jnp.bfloat16

time: 332 us -> 332 us (level)
    another operation x24 -> x25, local copies, waits for them, and re-layouts: 21 us -> 21 us
where the time goes in v1:
time: 332 us
  waiting for transfers between devices  100 us (30%)
  other arithmetic  84.9 us (26%)
  matrix products  56 us (17%)
  blocking collectives  46.4 us (14%)
  local copies, waits for them, and re-layouts  27.1 us (8%)
  between operations  13.4 us (4%)
    all_gather x2, waiting for transfers between devices, side_by_side(): out = lax.all_gather(both, axis, axis=dim, tiled=True)  88.7 us
    another operation x16, other arithmetic  40.8 us
    convert_element_type x8, other arithmetic, visit(): weights = jnp.where(causal, jnp.exp(jax.nn.log_sigmoid(scores) + later +...  37.1 us
    dot_general x8, matrix products, visit(): jnp.einsum('qhd,khd->hqk', query_heads, key_block, preferred_element_type...  36.4 us
    another operation x24, local copies, waits for them, and re-layouts  21 us
    all_to_all x1, blocking collectives, sum_at_owner(): lax.all_to_all(parts, axis, split_axis=0, concat_axis=0, tiled=True)  18.5 us
    all_to_all x1, blocking collectives, from_everyone(): lax.all_to_all(jnp.broadcast_to(x[None], (length, *x.shape)), axis, 0, 0,...  18.4 us
    ppermute x1, waiting for transfers between devices, from_behind(): return lax.ppermute(x, axis, pairs)  10.7 us
  transfers between devices with their start and end apart: 4, of which 2 were waited for; matrix products, arithmetic and copies ran while one was open for 49% of the time, Pallas kernels for 0%

profile of v1, /device:TPU:448, one launch (start us, length us, event | category | flops | bytes accessed | tf_op | source)
XLA Modules:
  0.0 331.5 jit_solution(5135130780065827146)
XLA Ops:
  10.5 88.7 %all-gather.4.cloned.1.call-done = bf16[16384,128]{0,1:T(8,128)(2,1)} async-done(((bf16[256,128]{0,1:T(8,128)(2,1)}), bf16[16384,128]{0,1:T(8,128)(2,1)}) %all-gather.4.cloned.1.call-update) | async-done | bytes 4194320 | tf_op jit(solution)/shard_map/all_gather | solution.py:13
  103.8 146.1 %while.13 = (s32[]{:T(128)}, f32[1,256,64]{1,2,0:T(8,128)S(1)}, f32[1,256]{1,0:T(1,128)S(1)}, s32[]{:T(128)}, s32[]{:T(128)}, /*index=5*/bf16[16384,1,64]{0,2,1:...) while((s32[]{:T(128)}, f32[1,256,64]{1,2,0:T(8,128)S(1)}, ...), condition=%wide.region_4.5_spmd.clone, body=%wide.region_0.4_spmd.clone.sunk | while | flops 219236352 | bytes 19711708 | solution.py:104
  103.8 4.6 %fusion.62 = (f32[256]{0:T(256)S(1)}, f32[256,2048]{0,1:T(8,128)S(1)}, f32[256,2048]{0,1:T(8,128)}) fusion(s32[256]{0:T(256)S(1)} %iota_add_fusion.4, s32[2048]{0:T(1024)S(1)} %iota_add_fusion.5, f32[]{:T(128)} %bitcast.71, bf16[256,1,64]{0,2,1:T(8,128)(2,1)S(1)} %get-tuple-element.219, bf16[16384,1,64]{0,2,1:T(8,128)(2,1)} %get-tuple-element.218, ...), kind=kOutput, calls=%fused_computation.31.clone.1 | convolution fusion | flops 73400064 | bytes 4499972 | tf_op jit(solution)/shard_map/while/body/qhd,khd->hqk/dot_general | solution.py:84
  108.4 5.0 %fusion.63 = f32[1,256,16,128]{1,2,3,0:T(8,128)S(1)} fusion(f32[1,256,16,128]{1,3,2,0:T(8,128)S(1)} %bitcast.75), kind=kOutput, calls=%fused_computation.16.clone.1 | output fusion | flops 66584576 | bytes 4194304 | tf_op jit(solution)/shard_map/reduce-window
  116.1 4.6 %fusion.64 = bf16[256,2048]{0,1:T(8,128)(2,1)S(1)} fusion(f32[1,256,16,128]{1,3,2,0:T(8,128)} %copy.34, f32[256,2048]{0,1:T(8,128)} %get-tuple-element.181, f32[256]{0:T(256)S(1)} %bitcast.80, f32[256,16]{0,1:T(8,128)S(1)} %slice_bitcast_fusion.7, s32[256]{0:T(256)S(1)} %iota_add_fusion.4, s32[2048]{0:T(1024)S(1)} %iota_add_fusion.5), kind=kLoop, calls=%fused_computation.8.clone.1 | loop fusion | flops 12058624 | bytes 5269504 | tf_op jit(solution)/shard_map/while/body/convert_element_type | solution.py:94
  126.6 5.0 %fusion.63 = f32[1,256,16,128]{1,2,3,0:T(8,128)S(1)} fusion(f32[1,256,16,128]{1,3,2,0:T(8,128)S(1)} %bitcast.75), kind=kOutput, calls=%fused_computation.16.clone.1 | output fusion | flops 66584576 | bytes 4194304 | tf_op jit(solution)/shard_map/reduce-window
  134.4 4.6 %fusion.64 = bf16[256,2048]{0,1:T(8,128)(2,1)S(1)} fusion(f32[1,256,16,128]{1,3,2,0:T(8,128)} %copy.34, f32[256,2048]{0,1:T(8,128)} %get-tuple-element.181, f32[256]{0:T(256)S(1)} %bitcast.80, f32[256,16]{0,1:T(8,128)S(1)} %slice_bitcast_fusion.7, s32[256]{0:T(256)S(1)} %iota_add_fusion.4, s32[2048]{0:T(1024)S(1)} %iota_add_fusion.5), kind=kLoop, calls=%fused_computation.8.clone.1 | loop fusion | flops 12058624 | bytes 5269504 | tf_op jit(solution)/shard_map/while/body/convert_element_type | solution.py:94
  144.9 5.0 %fusion.63 = f32[1,256,16,128]{1,2,3,0:T(8,128)S(1)} fusion(f32[1,256,16,128]{1,3,2,0:T(8,128)S(1)} %bitcast.75), kind=kOutput, calls=%fused_computation.16.clone.1 | output fusion | flops 66584576 | bytes 4194304 | tf_op jit(solution)/shard_map/reduce-window
  152.6 4.6 %fusion.64 = bf16[256,2048]{0,1:T(8,128)(2,1)S(1)} fusion(f32[1,256,16,128]{1,3,2,0:T(8,128)} %copy.34, f32[256,2048]{0,1:T(8,128)} %get-tuple-element.181, f32[256]{0:T(256)S(1)} %bitcast.80, f32[256,16]{0,1:T(8,128)S(1)} %slice_bitcast_fusion.7, s32[256]{0:T(256)S(1)} %iota_add_fusion.4, s32[2048]{0:T(1024)S(1)} %iota_add_fusion.5), kind=kLoop, calls=%fused_computation.8.clone.1 | loop fusion | flops 12058624 | bytes 5269504 | tf_op jit(solution)/shard_map/while/body/convert_element_type | solution.py:94
  163.1 5.0 %fusion.63 = f32[1,256,16,128]{1,2,3,0:T(8,128)S(1)} fusion(f32[1,256,16,128]{1,3,2,0:T(8,128)S(1)} %bitcast.75), kind=kOutput, calls=%fused_computation.16.clone.1 | output fusion | flops 66584576 | bytes 4194304 | tf_op jit(solution)/shard_map/reduce-window
  170.9 4.7 %fusion.64 = bf16[256,2048]{0,1:T(8,128)(2,1)S(1)} fusion(f32[1,256,16,128]{1,3,2,0:T(8,128)} %copy.34, f32[256,2048]{0,1:T(8,128)} %get-tuple-element.181, f32[256]{0:T(256)S(1)} %bitcast.80, f32[256,16]{0,1:T(8,128)S(1)} %slice_bitcast_fusion.7, s32[256]{0:T(256)S(1)} %iota_add_fusion.4, s32[2048]{0:T(1024)S(1)} %iota_add_fusion.5), kind=kLoop, calls=%fused_computation.8.clone.1 | loop fusion | flops 12058624 | bytes 5269504 | tf_op jit(solution)/shard_map/while/body/convert_element_type | solution.py:94
  176.9 4.6 %fusion.62 = (f32[256]{0:T(256)S(1)}, f32[256,2048]{0,1:T(8,128)S(1)}, f32[256,2048]{0,1:T(8,128)}) fusion(s32[256]{0:T(256)S(1)} %iota_add_fusion.4, s32[2048]{0:T(1024)S(1)} %iota_add_fusion.5, f32[]{:T(128)} %bitcast.71, bf16[256,1,64]{0,2,1:T(8,128)(2,1)S(1)} %get-tuple-element.219, bf16[16384,1,64]{0,2,1:T(8,128)(2,1)} %get-tuple-element.218, ...), kind=kOutput, calls=%fused_computation.31.clone.1 | convolution fusion | flops 73400064 | bytes 4499972 | tf_op jit(solution)/shard_map/while/body/qhd,khd->hqk/dot_general | solution.py:84
  181.5 5.0 %fusion.63 = f32[1,256,16,128]{1,2,3,0:T(8,128)S(1)} fusion(f32[1,256,16,128]{1,3,2,0:T(8,128)S(1)} %bitcast.75), kind=kOutput, calls=%fused_computation.16.clone.1 | output fusion | flops 66584576 | bytes 4194304 | tf_op jit(solution)/shard_map/reduce-window
  189.2 4.6 %fusion.64 = bf16[256,2048]{0,1:T(8,128)(2,1)S(1)} fusion(f32[1,256,16,128]{1,3,2,0:T(8,128)} %copy.34, f32[256,2048]{0,1:T(8,128)} %get-tuple-element.181, f32[256]{0:T(256)S(1)} %bitcast.80, f32[256,16]{0,1:T(8,128)S(1)} %slice_bitcast_fusion.7, s32[256]{0:T(256)S(1)} %iota_add_fusion.4, s32[2048]{0:T(1024)S(1)} %iota_add_fusion.5), kind=kLoop, calls=%fused_computation.8.clone.1 | loop fusion | flops 12058624 | bytes 5269504 | tf_op jit(solution)/shard_map/while/body/convert_element_type | solution.py:94
  199.7 5.0 %fusion.63 = f32[1,256,16,128]{1,2,3,0:T(8,128)S(1)} fusion(f32[1,256,16,128]{1,3,2,0:T(8,128)S(1)} %bitcast.75), kind=kOutput, calls=%fused_computation.16.clone.1 | output fusion | flops 66584576 | bytes 4194304 | tf_op jit(solution)/shard_map/reduce-window
  207.4 4.6 %fusion.64 = bf16[256,2048]{0,1:T(8,128)(2,1)S(1)} fusion(f32[1,256,16,128]{1,3,2,0:T(8,128)} %copy.34, f32[256,2048]{0,1:T(8,128)} %get-tuple-element.181, f32[256]{0:T(256)S(1)} %bitcast.80, f32[256,16]{0,1:T(8,128)S(1)} %slice_bitcast_fusion.7, s32[256]{0:T(256)S(1)} %iota_add_fusion.4, s32[2048]{0:T(1024)S(1)} %iota_add_fusion.5), kind=kLoop, calls=%fused_computation.8.clone.1 | loop fusion | flops 12058624 | bytes 5269504 | tf_op jit(solution)/shard_map/while/body/convert_element_type | solution.py:94
  217.9 5.0 %fusion.63 = f32[1,256,16,128]{1,2,3,0:T(8,128)S(1)} fusion(f32[1,256,16,128]{1,3,2,0:T(8,128)S(1)} %bitcast.75), kind=kOutput, calls=%fused_computation.16.clone.1 | output fusion | flops 66584576 | bytes 4194304 | tf_op jit(solution)/shard_map/reduce-window
  225.7 4.6 %fusion.64 = bf16[256,2048]{0,1:T(8,128)(2,1)S(1)} fusion(f32[1,256,16,128]{1,3,2,0:T(8,128)} %copy.34, f32[256,2048]{0,1:T(8,128)} %get-tuple-element.181, f32[256]{0:T(256)S(1)} %bitcast.80, f32[256,16]{0,1:T(8,128)S(1)} %slice_bitcast_fusion.7, s32[256]{0:T(256)S(1)} %iota_add_fusion.4, s32[2048]{0:T(1024)S(1)} %iota_add_fusion.5), kind=kLoop, calls=%fused_computation.8.clone.1 | loop fusion | flops 12058624 | bytes 5269504 | tf_op jit(solution)/shard_map/while/body/convert_element_type | solution.py:94
  236.2 5.0 %fusion.63 = f32[1,256,16,128]{1,2,3,0:T(8,128)S(1)} fusion(f32[1,256,16,128]{1,3,2,0:T(8,128)S(1)} %bitcast.75), kind=kOutput, calls=%fused_computation.16.clone.1 | output fusion | flops 66584576 | bytes 4194304 | tf_op jit(solution)/shard_map/reduce-window
  243.9 4.6 %fusion.64 = bf16[256,2048]{0,1:T(8,128)(2,1)S(1)} fusion(f32[1,256,16,128]{1,3,2,0:T(8,128)} %copy.34, f32[256,2048]{0,1:T(8,128)} %get-tuple-element.181, f32[256]{0:T(256)S(1)} %bitcast.80, f32[256,16]{0,1:T(8,128)S(1)} %slice_bitcast_fusion.7, s32[256]{0:T(256)S(1)} %iota_add_fusion.4, s32[2048]{0:T(1024)S(1)} %iota_add_fusion.5), kind=kLoop, calls=%fused_computation.8.clone.1 | loop fusion | flops 12058624 | bytes 5269504 | tf_op jit(solution)/shard_map/while/body/convert_element_type | solution.py:94
  250.2 9.5 %all_to_all.15 = bf16[8,2,1024]{2,1,0:T(2,128)(2,1)S(1)} all-to-all(bf16[8,2,1024]{2,1,0:T(2,128)(2,1)S(1)} %reshape.157), channel_id=1, replica_groups=mesh['sp'=64,'tp'=8] {'tp'}, dimensions={0} | all-to-all | bytes 65536 | tf_op jit(solution)/shard_map/all_to_all | solution.py:128
  261.7 18.4 %all_to_all.16 = bf16[8,32,2048]{2,1,0:T(8,128)(2,1)S(1)} all-to-all(bf16[8,32,2048]{2,1,0:T(8,128)(2,1)S(1)} %broadcast_in_dim.16), channel_id=1, replica_groups=mesh['sp'=64,'tp'=8] {'tp'}, dimensions={0} | all-to-all | bytes 2097152 | tf_op jit(solution)/shard_map/all_to_all | solution.py:25
  289.6 10.7 %collective-permute-done = bf16[2,1408]{0,1:T(8,128)(2,1)S(1)} collective-permute-done((bf16[2,1408]{0,1:T(8,128)(2,1)S(1)}, bf16[2,1408]{0,1:T(8,128)(2,1)S(1)}, u32[]{:S(2)}, u32[]{:S(2)}) %collective-permute-start) | collective-permute-done | bytes 5664 | tf_op jit(solution)/shard_map/ppermute | solution.py:35
  305.4 18.5 %all_to_all.17 = bf16[8,32,2048]{2,1,0:T(8,128)(2,1)S(1)} all-to-all(bf16[8,32,2048]{2,1,0:T(8,128)(2,1)S(1)} %bitcast.78), channel_id=1, replica_groups=mesh['sp'=64,'tp'=8] {'tp'}, dimensions={0} | all-to-all | bytes 2097152 | tf_op jit(solution)/shard_map/all_to_all | solution.py:45
  (136 shorter events, 85.1 us)
Async XLA Ops:
  6.5 253.4 %copy-start = (bf16[512,2048]{1,0:T(8,128)(2,1)S(1)}, bf16[512,2048]{1,0:T(8,128)(2,1)}, u32[]{:S(2)}) copy-start(bf16[512,2048]{1,0:T(8,128)(2,1)} %param.21) | copy-start | bytes 6291460
  6.5 92.7 %all-gather.4.cloned.1.call-start = ((), (), s32[]{:S(2)}) async-start(), calls=%async_computation.3 | async-start | bytes 4259840 | tf_op jit(solution)/shard_map/all_gather | solution.py:13
  8.1 272.0 %all-gather.6.cloned.1.call-start = ((), (), s32[]{:S(2)}) async-start(), calls=%async_computation.4 | async-start | bytes 5857280 | tf_op jit(solution)/shard_map/all_gather | solution.py:13
  9.7 292.6 %all-gather.8.cloned.1.call-start = ((), (), s32[]{:S(2)}) async-start(), calls=%async_computation.5 | async-start | bytes 3194880 | tf_op jit(solution)/shard_map/all_gather | solution.py:55
  10.5 93.3 %copy-start.10 = (bf16[256,64]{0,1:T(8,128)(2,1)S(1)}, bf16[256,64]{0,1:T(8,128)(2,1)}, u32[]{:S(2)}) copy-start(bf16[256,64]{0,1:T(8,128)(2,1)} %param.16) | copy-start | bytes 98308
  249.9 10.7 %copy-start.3 = (bf16[32,2048]{1,0:T(8,128)(2,1)S(1)}, bf16[32,2048]{1,0:T(8,128)(2,1)}, u32[]{:S(2)}) copy-start(bf16[32,2048]{1,0:T(8,128)(2,1)} %param.20) | copy-start | bytes 393220
  249.9 10.7 %copy-start.6 = (f32[2048]{0:T(1024)S(1)}, f32[2048]{0:T(1024)}, u32[]{:S(2)}) copy-start(f32[2048]{0:T(1024)} %param.22) | copy-start | bytes 24580
  249.9 11.6 %copy-start.7 = (f32[2048]{0:T(1024)S(1)}, f32[2048]{0:T(1024)}, u32[]{:S(2)}) copy-start(f32[2048]{0:T(1024)} %param.23) | copy-start | bytes 24580
  260.8 0.7 copy-start.1
  280.1 3.6 %copy-start.9 = (bf16[2048,1408]{1,0:T(8,128)(2,1)S(1)}, bf16[2048,1408]{1,0:T(8,128)(2,1)}, u32[]{:S(2)}) copy-start(bf16[2048,1408]{1,0:T(8,128)(2,1)} %all-gather.6.cloned.1.call-done) | copy-start | bytes 17301508
  283.7 5.8 %copy-start.4 = (f32[3,704]{1,0:T(4,128)S(1)}, f32[3,704]{1,0:T(4,128)}, u32[]{:S(2)}) copy-start(f32[3,704]{1,0:T(4,128)} %param.27) | copy-start | bytes 25348
  283.7 5.8 %copy-start.5 = (f32[3,704]{1,0:T(4,128)S(1)}, f32[3,704]{1,0:T(4,128)}, u32[]{:S(2)}) copy-start(f32[3,704]{1,0:T(4,128)} %param.26) | copy-start | bytes 25348
  286.6 13.8 %collective-permute-start = (bf16[2,1408]{0,1:T(8,128)(2,1)S(1)}, bf16[2,1408]{0,1:T(8,128)(2,1)S(1)}, u32[]{:S(2)}, u32[]{:S(2)}) collective-permute-start(bf16[2,1408]{0,1:T(8,128)(2,1)S(1)} %pad_maximum_fusion), channel_id=1, source_target_pairs={{0,8},{8,16},{16,24},{24,32},{32,40},{40,48},{48,56},{56,64},{64,7... | collective-permute-start | bytes 16904 | tf_op jit(solution)/shard_map/ppermute | solution.py:35
  305.3 18.9 %copy-start.2 = (bf16[32,2048]{1,0:T(8,128)(2,1)S(1)}, bf16[32,2048]{1,0:T(8,128)(2,1)}, u32[]{:S(2)}) copy-start(bf16[32,2048]{1,0:T(8,128)(2,1)} %copy-done.1) | copy-start | bytes 393220
  305.4 18.8 %copy-start.8 = (f32[2048]{0:T(1024)S(1)}, f32[2048]{0:T(1024)}, u32[]{:S(2)}) copy-start(f32[2048]{0:T(1024)} %param.29) | copy-start | bytes 24580
Sparse Core Ops, SparseCore 0:
  10.3 88.8 all-gather.3
  102.2 85.3 all-gather.5
  190.6 82.1 all-gather.7
